TPU v7x, 32 devices: a whole 2x2x4 slice. The times are simulated.
32 devices in a mesh: ep: 8 (over z, core), tp: 4 (over y, x).
Axes of the slice: x: 2, y: 2, z: 4, core: 2. Of those that a mesh axis runs over, the one named last changes fastest.
Arguments:
- tokens: bfloat16 [512, 4096], P('ep', 'tp'), may hold values from -600 to 600
- in_gain: float32 [4096], P('tp'), may hold values from 0.1 to 1.9
- out_gain: float32 [4096], P('tp'), may hold values from 0.1 to 1.9
- routes: int32 [512, 4], replicated, may hold values from 0 to 31, as said below
- route_weights: float32 [512, 4], replicated, may hold values from 0.05 to 1
- w_gate: bfloat16 [32, 4096, 1024], P('ep', 'tp'), may hold values from -0.09375 to 0.09375
- w_up: bfloat16 [32, 4096, 1024], P('ep', 'tp'), may hold values from -0.09375 to 0.09375
- w_down: bfloat16 [32, 1024, 4096], P('ep', None, 'tp'), may hold values from -0.375 to 0.375
Outputs:
- result: bfloat16 [512, 4096], P('ep', 'tp')
Inputs may be any that keep to these rules, and one draw needn't show every extreme that they name: `routes`: each row names 4 different experts, all in one group of 8 consecutive numbers. In the rows of one index of ep (aligned blocks of 64 rows) no expert is named by more than 16 rows, and some expert by exactly 16.
All inputs are finite; a program needn't handle non-finite values.
Results may differ from a plain program's by a relative error of at most 0.025.
Values may be sent and summed in bfloat16 or wider, within the bound.
A program may use at most 64 MiB of HBM per device.

v0:
```python
import jax
import jax.numpy as jnp
from jax import lax
from jax.sharding import PartitionSpec as P

D = 4096


EPS = 1e-06


def run_experts(slot_rows, w_gate, w_up, w_down):
    gate_part = jnp.einsum(
        "secd,edf->secf", slot_rows, w_gate, preferred_element_type=jnp.float32
    ).astype(jnp.bfloat16)
    up_part = jnp.einsum(
        "secd,edf->secf", slot_rows, w_up, preferred_element_type=jnp.float32
    ).astype(jnp.bfloat16)
    gate_sum, up_sum = (
        lax.psum(gate_part, "tp").astype(jnp.float32),
        lax.psum(up_part, "tp").astype(jnp.float32),
    )
    active = (jax.nn.silu(gate_sum) * up_sum).astype(jnp.bfloat16)
    return jnp.einsum("secf,efd->secd", active, w_down, preferred_element_type=jnp.float32).astype(
        jnp.bfloat16
    )


def on_device(tokens, in_gain, out_gain, routes, route_weights, w_gate, w_up, w_down):
    tok_rows, local_width = tokens.shape
    top_count = routes.shape[1]
    local_experts = w_gate.shape[0]
    groups_ep = lax.axis_size("ep")
    experts = local_experts * groups_ep
    capacity = max(2, 2 * tok_rows * top_count // experts)
    values = tokens.astype(jnp.float32)
    sum_squares = lax.psum(jnp.sum(values * values, axis=1), "tp")
    normed = (values * lax.rsqrt(sum_squares / D + EPS)[:, None] * in_gain).astype(jnp.bfloat16)
    row_start = lax.axis_index("ep") * tok_rows
    my_routes = lax.dynamic_slice_in_dim(routes, row_start, tok_rows, 0)
    my_weights = lax.dynamic_slice_in_dim(route_weights, row_start, tok_rows, 0)
    flat_ids = my_routes.reshape(-1)
    matches = (flat_ids[:, None] == jnp.arange(experts, dtype=jnp.int32)[None, :]).astype(jnp.int32)
    slot_rank = jnp.sum((jnp.cumsum(matches, axis=0) - matches) * matches, axis=1)
    position = flat_ids * capacity + slot_rank
    dispatch_table = jnp.any(
        position.reshape(tok_rows, top_count, 1)
        == jnp.arange(experts * capacity, dtype=jnp.int32)[None, None, :],
        axis=1,
    )
    outgoing = jnp.einsum(
        "ts,td->sd", dispatch_table.astype(jnp.bfloat16), normed, preferred_element_type=jnp.float32
    ).astype(jnp.bfloat16)
    outgoing = outgoing.reshape(groups_ep, local_experts, capacity, local_width)
    answers = run_experts(
        lax.all_to_all(outgoing, "ep", split_axis=0, concat_axis=0, tiled=True),
        w_gate,
        w_up,
        w_down,
    )
    returned = lax.all_to_all(answers, "ep", split_axis=0, concat_axis=0, tiled=True)
    flat_out = returned.reshape(experts * capacity, local_width)
    picked = flat_out[position].reshape(tok_rows, top_count, local_width)
    combined = jnp.sum(my_weights[:, :, None] * picked.astype(jnp.float32), axis=1)
    out_squares = lax.psum(jnp.sum(combined * combined, axis=1), "tp")
    return (combined * lax.rsqrt(out_squares / D + EPS)[:, None] * out_gain).astype(jnp.bfloat16)


def solution(mesh):
    placed = (
        P("ep", "tp"),
        P("tp"),
        P("tp"),
        P(),
        P(),
        P("ep", "tp", None),
        P("ep", "tp", None),
        P("ep", None, "tp"),
    )
    return jax.shard_map(
        on_device, mesh=mesh, in_specs=placed, out_specs=P("ep", "tp"), check_vma=False
    )
```

profile of v0, /device:TPU:0, one launch (start us, length us, event | category | flops | bytes accessed | tf_op | source)
XLA Modules:
  0.0 185.9 jit_solution(116999732136430107)
XLA Ops:
  6.5 0.0 copy-start
  6.5 0.0 all-reduce.3.cloned.1.call-start
  6.5 0.7 copy-done
  7.2 0.1 constant_dynamic-slice_fusion
  7.3 0.1 copy.33
  7.4 0.1 eq.42
  7.5 0.1 eq.38
  7.6 0.6 reduce-window.6
  8.2 0.2 slice_reduce_fusion
  8.5 0.1 fusion.42
  8.6 0.1 reduce_sum.41
  8.7 0.1 copy.26
  8.8 0.1 fusion.33
  8.9 1.0 fusion.34
  10.0 11.4 %psum.28 = f32[64]{0:T(128)S(1)} all-reduce(f32[64]{0:T(128)S(1)} %fusion.34), channel_id=1, replica_groups=mesh['ep'=8,'tp'=4] {'tp'}, use_global_device_ids=true, to_apply=%region_5.6 | all-reduce | flops 64 | bytes 512 | tf_op jit(solution)/shard_map/psum | solution.py:37
  21.4 1.4 convolution_convert_fusion
  22.8 31.2 %all_to_all.10 = bf16[8,4,16,1024]{3,2,1,0:T(8,128)(2,1)S(1)} all-to-all(bf16[8,4,16,1024]{3,2,1,0:T(8,128)(2,1)S(1)} %bitcast.58), channel_id=1, replica_groups=mesh['ep'=8,'tp'=4] {'ep'}, dimensions={0} | all-to-all | bytes 2097152 | tf_op jit(solution)/shard_map/all_to_all | solution.py:56
  54.0 0.0 copy-start.1
  54.0 5.9 %fusion.23 = bf16[8,4,16,1024]{3,2,0,1:T(8,128)(2,1)} fusion(bf16[4,1024,1024]{2,1,0:T(8,128)(2,1)} %param.14, bf16[8,4,16,1024]{3,2,1,0:T(8,128)(2,1)S(1)} %all_to_all.10), kind=kOutput, calls=%fused_computation.19 | convolution fusion | flops 1074266112 | bytes 10485760 | tf_op jit(solution)/shard_map/secd,edf->secf/dot_general | solution.py:16
  59.9 0.0 copy-done.1
  59.9 2.3 %fusion.26 = bf16[8,4,16,1024]{3,2,0,1:T(8,128)(2,1)} fusion(bf16[4,1024,1024]{2,1,0:T(8,128)(2,1)S(1)} %copy-done.1, bf16[8,4,16,1024]{3,2,1,0:T(8,128)(2,1)S(1)} %all_to_all.10), kind=kOutput, calls=%fused_computation.20 | convolution fusion | flops 1074266112 | bytes 10485760 | tf_op jit(solution)/shard_map/secd,edf->secf/dot_general | solution.py:13
  62.1 0.0 all-reduce.3.cloned.1.call-update
  62.2 66.7 %all-reduce.3.cloned.1.call-done = (bf16[8,4,16,1024]{3,2,0,1:T(8,128)(2,1)}, bf16[8,4,16,1024]{3,2,0,1:T(8,128)(2,1)}) async-done(((bf16[8,4,16,1024]{3,2,0,1:T(8,128)(2,1)}, bf16[8,4,16,1024]{3,2,0,1:T(8,128)(2,1)}), (bf16[8,4,16,1024]{3,2,0,1:T(8,128)(2,1)}, bf16[8,4,16,1024]{3,2,0,1:T(8,128)(2,1)})) %all-reduce.3.cloned.1.call-update) | async-done | bytes 2097168 | tf_op jit(solution)/shard_map/psum | solution.py:21
  128.9 5.9 %fusion.20 = bf16[8,4,16,1024]{3,2,0,1:T(8,128)(2,1)S(1)} fusion(bf16[4,1024,1024]{2,1,0:T(8,128)(2,1)} %param.15, bf16[8,4,16,1024]{3,2,0,1:T(8,128)(2,1)} %get-tuple-element.5, bf16[8,4,16,1024]{3,2,0,1:T(8,128)(2,1)} %get-tuple-element.6), kind=kOutput, calls=%fused_computation.18 | convolution fusion | flops 1078460416 | bytes 11534336 | tf_op jit(solution)/shard_map/secf,efd->secd/dot_general | solution.py:24
  134.8 1.1 copy.29
  135.9 4.6 %all-to-all-start.1 = ((bf16[8,4,16,1024]{3,2,1,0:T(8,128)(2,1)}), bf16[8,4,16,1024]{3,2,1,0:T(8,128)(2,1)S(1)}, u32[]{:S(2)}, u32[]{:S(2)}) async-start(bf16[8,4,16,1024]{3,2,1,0:T(8,128)(2,1)} %copy.29), calls=%async_computation.1 | async-start | bytes 2097152 | tf_op jit(solution)/shard_map/all_to_all | solution.py:61
  140.5 0.1 mul.89
  140.6 0.8 constant_dynamic-slice_fusion.1
  141.3 0.1 copy.23
  141.5 25.6 %all-to-all-done.1 = bf16[8,4,16,1024]{3,2,1,0:T(8,128)(2,1)S(1)} async-done(((bf16[8,4,16,1024]{3,2,1,0:T(8,128)(2,1)}), bf16[8,4,16,1024]{3,2,1,0:T(8,128)(2,1)S(1)}, u32[]{:S(2)}, u32[]{:S(2)}) %all-to-all-start.1) | async-done | bytes 1048608 | tf_op jit(solution)/shard_map/all_to_all | solution.py:61
  167.0 1.2 gather_fusion
  168.2 0.0 copy-start.2
  168.2 0.3 reshape.70
  168.6 0.7 multiply_reduce_fusion
  169.3 0.1 multiply_reduce_fusion.1
  169.4 8.9 %psum.31 = f32[64]{0:T(128)S(1)} all-reduce(f32[64]{0:T(128)S(1)} %multiply_reduce_fusion.1), channel_id=1, replica_groups=mesh['ep'=8,'tp'=4] {'tp'}, use_global_device_ids=true, to_apply=%region_10.11 | all-reduce | flops 64 | bytes 512 | tf_op jit(solution)/shard_map/psum | solution.py:65
  178.3 0.0 copy-done.2
  178.3 0.8 multiply_convert_fusion
  (8 shorter events, 0.1 us)
Async XLA Ops:
  6.5 0.7 copy-start
  6.5 122.3 %all-reduce.3.cloned.1.call-start = ((), (), s32[]{:S(2)}) async-start(), calls=%async_computation.2 | async-start | bytes 4194304 | tf_op jit(solution)/shard_map/psum | solution.py:21
  54.0 5.9 %copy-start.1 = (bf16[4,1024,1024]{2,1,0:T(8,128)(2,1)S(1)}, bf16[4,1024,1024]{2,1,0:T(8,128)(2,1)}, u32[]{:S(2)}) copy-start(bf16[4,1024,1024]{2,1,0:T(8,128)(2,1)} %param.13) | copy-start | bytes 25165828
  135.9 31.2 %all-to-all-start.1 = ((bf16[8,4,16,1024]{3,2,1,0:T(8,128)(2,1)}), bf16[8,4,16,1024]{3,2,1,0:T(8,128)(2,1)S(1)}, u32[]{:S(2)}, u32[]{:S(2)}) async-start(bf16[8,4,16,1024]{3,2,1,0:T(8,128)(2,1)} %copy.29), calls=%async_computation.1 | async-start | bytes 2097152 | tf_op jit(solution)/shard_map/all_to_all | solution.py:61
  168.2 10.1 %copy-start.2 = (f32[1024]{0:T(1024)S(1)}, f32[1024]{0:T(1024)}, u32[]{:S(2)}) copy-start(f32[1024]{0:T(1024)} %param.10) | copy-start | bytes 12292
Sparse Core Ops, SparseCore 0:
  62.3 66.5 all-reduce.2
where the time goes:
time: 186 us
  waiting for transfers between devices  92.3 us (50%)
  blocking collectives  51.6 us (28%)
  matrix products  15.4 us (8%)
  between operations  13.5 us (7%)
  local copies, waits for them, and re-layouts  5.01 us (3%)
  starting transfers between devices  4.61 us (2%)
  other arithmetic  3.53 us (2%)
    psum x1, waiting for transfers between devices, run_experts(): lax.psum(up_part, 'tp').astype(jnp.float32)  66.7 us
    all_to_all x1, blocking collectives, on_device(): lax.all_to_all(outgoing, 'ep', split_axis=0, concat_axis=0, tiled=True)  31.2 us
    all_to_all x1, waiting for transfers between devices, on_device(): lax.all_to_all(answers, 'ep', split_axis=0, concat_axis=0, tiled=True)  25.6 us
    psum x1, blocking collectives, on_device(): sum_squares = lax.psum(jnp.sum(values * values, axis=1), 'tp')  11.4 us
    psum x1, blocking collectives, on_device(): out_squares = lax.psum(jnp.sum(combined * combined, axis=1), 'tp')  8.93 us
    dot_general x1, matrix products, run_experts(): jnp.einsum('secf,efd->secd', active, w_down, preferred_element_type=jnp.f...  5.89 us
    dot_general x1, matrix products, run_experts(): jnp.einsum('secd,edf->secf', slot_rows, w_up, preferred_element_type=jnp....  5.86 us
    all_to_all x1, starting transfers between devices, on_device(): lax.all_to_all(answers, 'ep', split_axis=0, concat_axis=0, tiled=True)  4.61 us
  transfers between devices with their start and end apart: 2, of which 2 were waited for; matrix products, arithmetic and copies ran while one was open for 1% of the time, Pallas kernels for 0%

commit v1 on v0

--- a/solution.py
+++ b/solution.py
@@ -1,12 +1,434 @@
+import functools
+
 import jax
 import jax.numpy as jnp
 from jax import lax
+from jax.experimental import pallas as pl
+from jax.experimental.pallas import tpu as pltpu
 from jax.sharding import PartitionSpec as P
 
 D = 4096
-
+GROUP = 8
 
 EPS = 1e-06
+MESH = pl.DeviceIdType.MESH
+F32, BF16 = jnp.float32, jnp.bfloat16
+
+
+def iota(shape, dim):
+    return lax.broadcasted_iota(jnp.int32, shape, dim)
+
+
+def tdot(a, b):
+    return lax.dot_general(a, b, (((0,), (0,)), ((), ())), preferred_element_type=F32)
+
+
+def kernel(
+    cfg,
+    tokens_ref,
+    in_gain_ref,
+    out_gain_ref,
+    routes_ref,
+    weights_ref,
+    wg_hbm,
+    wu_hbm,
+    wd_hbm,
+    out_ref,
+    wg,
+    wu,
+    wd,
+    pick,
+    slot_w,
+    own_pick,
+    ss_out,
+    ss_in,
+    send_rows,
+    compact,
+    part,
+    s1_in,
+    keep,
+    s2_out,
+    s2_in,
+    act,
+    comb,
+    x_out,
+    x_in,
+    r_out,
+    r_in,
+    w_sem,
+    ss_send,
+    ss_recv,
+    d_send,
+    f_send,
+    d_recv,
+    s1_send,
+    s1_recv,
+    s2_send,
+    s2_recv,
+    g1_send,
+    g1_recv,
+    g2_send,
+    g2_recv,
+    x_send,
+    x_recv,
+    r_send,
+    r_recv,
+):
+    n_ep, n_z, tok, n_exp, cap, width, ff, top = cfg
+    rows_z = cap * GROUP // top
+    tok_all = n_ep * tok
+    me = lax.axis_index("ep")
+    tp = lax.axis_index("tp")
+    z, core = me // 2, lax.rem(me, 2)
+    other = 1 - core
+    y, x = tp // 2, lax.rem(tp, 2)
+    x_tp = 2 * y + (1 - x)
+    y_tp = 2 * (1 - y) + x
+    xy_tp = 2 * (1 - y) + (1 - x)
+    partner = 2 * z + other
+    peers = (x_tp, y_tp, xy_tp)
+
+    for j in range(n_exp):
+        pltpu.make_async_copy(wg_hbm.at[j], wg.at[j], w_sem.at[0, j]).start()
+        pltpu.make_async_copy(wu_hbm.at[j], wu.at[j], w_sem.at[1, j]).start()
+    for j in range(n_exp):
+        pltpu.make_async_copy(wd_hbm.at[j], wd.at[j], w_sem.at[2, j]).start()
+
+    def far_ep(dz):
+        return 2 * lax.rem(z + dz, n_z) + core
+
+    barrier = pltpu.get_barrier_semaphore()
+    for peer in peers:
+        pl.semaphore_signal(barrier, inc=1, device_id={"tp": peer}, device_id_type=MESH)
+    pl.semaphore_signal(barrier, inc=1, device_id={"ep": partner}, device_id_type=MESH)
+    for dz in range(1, n_z):
+        pl.semaphore_signal(barrier, inc=1, device_id={"ep": far_ep(dz)}, device_id_type=MESH)
+
+    def remote(src, dst, send, recv, axis, dev):
+        return pltpu.make_async_remote_copy(
+            src_ref=src,
+            dst_ref=dst,
+            send_sem=send,
+            recv_sem=recv,
+            device_id={axis: dev},
+            device_id_type=MESH,
+        )
+
+    def square_copy(which, k):
+        return remote(
+            ss_out.at[which],
+            ss_in.at[which, k],
+            ss_send.at[which, k],
+            ss_recv.at[which, k],
+            "tp",
+            peers[k],
+        )
+
+    values = tokens_ref[...].astype(F32)
+    square = jnp.sum(values * values, axis=1, keepdims=True)
+    ss_out[0] = jnp.broadcast_to(square, (tok, 128))
+
+    lane = iota((tok, 128), 1)
+    own_routes = routes_ref[pl.ds(me * tok, tok), :]
+    group = own_routes[:, 0:1] // GROUP
+    in_group = (lane == group).astype(F32)
+    before = (iota((tok, tok), 1) < iota((tok, tok), 0)).astype(BF16)
+    ranks = jnp.dot(before, in_group.astype(BF16), preferred_element_type=F32)
+    rank = jnp.sum(ranks * in_group, axis=1, keepdims=True).astype(jnp.int32)
+    own_lane = iota((tok, n_z * rows_z), 1)
+    own_pick[...] = (own_lane == group * rows_z + rank).astype(BF16)
+
+    pl.semaphore_wait(barrier, 4 + n_z - 1)
+    for k in range(3):
+        square_copy(0, k).start()
+
+    routes = routes_ref[...]
+    lane = iota((tok_all, 128), 1)
+    row_block = iota((tok_all, 128), 0) // tok
+    first = me * n_exp
+    hits = jnp.where((lane == n_exp) & (routes[:, 0:1] // GROUP == z), 1.0, 0.0)
+    wt = jnp.zeros((tok_all, 128), F32)
+    for k in range(top):
+        match = (routes[:, k : k + 1] == first + lane) & (lane < n_exp)
+        hits = hits + jnp.where(match, 1.0, 0.0)
+        wt = wt + jnp.where(match, weights_ref[:, k : k + 1], 0.0)
+    t_row, t_col = iota((tok_all, tok_all), 0), iota((tok_all, tok_all), 1)
+    before = ((t_col < t_row) & (t_col // tok == t_row // tok)).astype(BF16)
+    ranks = jnp.dot(before, hits.astype(BF16), preferred_element_type=F32)
+    rank = jnp.where(hits > 0.0, ranks, -1.0).astype(jnp.int32)
+    wide = iota((tok_all, n_ep * rows_z), 1)
+    wide_block = iota((tok_all, n_ep * rows_z), 0) // tok
+    group_rows = (
+        (rank[:, n_exp : n_exp + 1] == wide % rows_z) & (wide // rows_z == wide_block)
+    ).astype(BF16)
+    w_hi = wt.astype(BF16)
+    w_mid = (wt - w_hi.astype(F32)).astype(BF16)
+    w_lo = (wt - w_hi.astype(F32) - w_mid.astype(F32)).astype(BF16)
+    slots = n_ep * cap
+    for j in range(n_exp):
+        slot = (
+            (rank[:, j : j + 1] == lane % cap) & (lane // cap == row_block)
+        ).astype(BF16)
+        pick[j] = tdot(slot, group_rows).astype(BF16)
+        weight = tdot(slot, w_hi) + tdot(slot, w_mid) + tdot(slot, w_lo)
+        weight = jnp.sum(jnp.where(iota((slots, 128), 1) == j, weight, 0.0), axis=1, keepdims=True)
+        slot_w[j] = jnp.broadcast_to(weight, (slots, 128)).reshape(n_ep, cap, 128)
+
+    for k in range(3):
+        square_copy(0, k).wait_recv()
+    square = ss_out[0] + ss_in[0, 0] + ss_in[0, 1] + ss_in[0, 2]
+    scale = lax.rsqrt(square[:, 0:1] / D + EPS)
+    normed = (values * scale * in_gain_ref[...]).astype(BF16)
+    send_rows[...] = tdot(own_pick[...], normed).astype(BF16).reshape(n_z, rows_z, width)
+
+    def dispatch(dz, src_block, far):
+        return remote(
+            send_rows.at[lax.rem(z + dz, n_z)],
+            compact.at[src_block],
+            d_send.at[dz - 1],
+            d_recv.at[src_block],
+            "ep",
+            far,
+        )
+
+    def forward(k, block):
+        return remote(
+            compact.at[block], compact.at[block], f_send.at[k], d_recv.at[block], "ep", partner
+        )
+
+    for dz in range(1, n_z):
+        dispatch(dz, me, far_ep(dz)).start()
+    compact[me] = send_rows[z]
+    own_forward = remote(
+        send_rows.at[z], compact.at[me], f_send.at[0], d_recv.at[me], "ep", partner
+    )
+    own_forward.start()
+    for dz in range(1, n_z):
+        block = 2 * lax.rem(z - dz + n_z, n_z) + core
+        dispatch(dz, block, far_ep(dz)).wait_recv()
+        forward(dz, block).start()
+    for dz in range(n_z):
+        block = 2 * lax.rem(z - dz + n_z, n_z) + other
+        forward(0, block).wait_recv()
+
+    half = n_ep // 2
+
+    def side(h):
+        return (x_tp, y_tp, x, y) if h == 0 else (y_tp, x_tp, y, x)
+
+    def s1(j, h):
+        near, _, a, _ = side(h)
+        return remote(
+            part.at[j, pl.ds(h * half + 2 * (1 - a), 2)],
+            s1_in.at[j, h],
+            s1_send.at[j, h],
+            s1_recv.at[j, h],
+            "tp",
+            near,
+        )
+
+    def s2(j, h):
+        return remote(
+            s2_out.at[j, h], s2_in.at[j, h], s2_send.at[j, h], s2_recv.at[j, h], "tp", side(h)[1]
+        )
+
+    def g1(j, h):
+        _, near, a, b = side(h)
+        piece = act.at[j, h * half + 2 * a + b]
+        return remote(piece, piece, g1_send.at[j, h], g1_recv.at[j, h], "tp", near)
+
+    def g2(j, h):
+        near, _, a, _ = side(h)
+        piece = act.at[j, pl.ds(h * half + 2 * a, 2)]
+        return remote(piece, piece, g2_send.at[j, h], g2_recv.at[j, h], "tp", near)
+
+    def w_wait(k, j, hbm, vmem):
+        pltpu.make_async_copy(hbm.at[j], vmem.at[j], w_sem.at[k, j]).wait()
+
+    @pl.loop(0, n_exp)
+    def _(j):
+        rows = jnp.dot(
+            pick[j], compact[...].reshape(n_ep * rows_z, width), preferred_element_type=F32
+        ).astype(BF16)
+        w_wait(0, j, wg_hbm, wg)
+        part[j, :, :, 0:ff] = (
+            jnp.dot(rows, wg[j], preferred_element_type=F32).astype(BF16).reshape(n_ep, cap, ff)
+        )
+        w_wait(1, j, wu_hbm, wu)
+        part[j, :, :, ff : 2 * ff] = (
+            jnp.dot(rows, wu[j], preferred_element_type=F32).astype(BF16).reshape(n_ep, cap, ff)
+        )
+        for h in range(2):
+            s1(j, h).start()
+
+    @pl.loop(0, n_exp)
+    def _(j):
+        for h in range(2):
+            _, _, a, b = side(h)
+            s1(j, h).wait_recv()
+            mine = h * half + 2 * a
+            s2_out[j, h] = (
+                part[j, mine + 1 - b].astype(F32) + s1_in[j, h, 1 - b].astype(F32)
+            ).astype(BF16)
+            s2(j, h).start()
+            keep[j, h] = part[j, mine + b].astype(F32) + s1_in[j, h, b].astype(F32)
+
+    @pl.loop(0, n_exp)
+    def _(j):
+        for h in range(2):
+            _, _, a, b = side(h)
+            s2(j, h).wait_recv()
+            piece = h * half + 2 * a + b
+            total = keep[j, h] + s2_in[j, h].astype(F32)
+            gate, up = total[:, 0:ff], total[:, ff : 2 * ff]
+            act[j, piece] = (
+                gate / (1.0 + jnp.exp(-gate)) * up * slot_w[j, piece][:, 0:1]
+            ).astype(BF16)
+            g1(j, h).start()
+
+    @pl.loop(0, n_exp)
+    def _(j):
+        for h in range(2):
+            g1(j, h).wait_recv()
+            g2(j, h).start()
+
+    comb[...] = jnp.zeros_like(comb)
+
+    @pl.loop(0, n_exp)
+    def _(j):
+        w_wait(2, j, wd_hbm, wd)
+        for h in range(2):
+            g2(j, h).wait_recv()
+        result = jnp.dot(
+            act[j].reshape(slots, ff), wd[j], preferred_element_type=F32
+        ).astype(BF16)
+        comb[...] += tdot(pick[j], result).reshape(n_z, 2, rows_z, width)
+
+    def swap(k):
+        return remote(x_out.at[k], x_in.at[k], x_send.at[k], x_recv.at[k], "ep", partner)
+
+    def home(dz, far):
+        return remote(
+            r_out.at[dz], r_in.at[z], r_send.at[dz - 1], r_recv.at[z], "ep", far
+        )
+
+    def home_in(dz):
+        block = lax.rem(z - dz + n_z, n_z)
+        return remote(
+            r_out.at[dz], r_in.at[block], r_send.at[dz - 1], r_recv.at[block], "ep", far_ep(dz)
+        )
+
+    for dz in range(1, n_z + 1):
+        k = dz % n_z
+        x_out[k] = comb[lax.rem(z + dz, n_z), other].astype(BF16)
+        swap(k).start()
+    for dz in range(1, n_z + 1):
+        k = dz % n_z
+        mine = comb[lax.rem(z + dz, n_z), core]
+        swap(k).wait_recv()
+        total = (mine + x_in[k].astype(F32)).astype(BF16)
+        if k:
+            r_out[k] = total
+            home(k, far_ep(k)).start()
+        else:
+            r_in[z] = total
+    for dz in range(1, n_z):
+        home_in(dz).wait_recv()
+
+    combined = jnp.dot(
+        own_pick[...], r_in[...].reshape(n_z * rows_z, width), preferred_element_type=F32
+    )
+    square = jnp.sum(combined * combined, axis=1, keepdims=True)
+    ss_out[1] = jnp.broadcast_to(square, (tok, 128))
+    for k in range(3):
+        square_copy(1, k).start()
+    for k in range(3):
+        square_copy(1, k).wait_recv()
+    square = ss_out[1] + ss_in[1, 0] + ss_in[1, 1] + ss_in[1, 2]
+    scale = lax.rsqrt(square[:, 0:1] / D + EPS)
+    out_ref[...] = (combined * scale * out_gain_ref[...]).astype(BF16)
+
+    for k in range(3):
+        square_copy(0, k).wait_send()
+        square_copy(1, k).wait_send()
+    own_forward.wait_send()
+    for dz in range(1, n_z):
+        dispatch(dz, me, far_ep(dz)).wait_send()
+        forward(dz, me).wait_send()
+        home(dz, far_ep(dz)).wait_send()
+    for k in range(n_z):
+        swap(k).wait_send()
+
+    @pl.loop(0, n_exp)
+    def _(j):
+        for h in range(2):
+            s1(j, h).wait_send()
+            s2(j, h).wait_send()
+            g1(j, h).wait_send()
+            g2(j, h).wait_send()
+
+
+def fused(mesh, tokens, in_gain, out_gain, routes, route_weights, w_gate, w_up, w_down):
+    tok, width = tokens.shape
+    top = routes.shape[1]
+    n_exp, _, ff = w_gate.shape
+    n_ep = mesh.shape["ep"]
+    n_z = n_ep // 2
+    cap = max(2, 2 * tok * top // (n_exp * n_ep))
+    rows_z = cap * GROUP // top
+    cfg = (n_ep, n_z, tok, n_exp, cap, width, ff, top)
+    vmem = pl.BlockSpec(memory_space=pltpu.VMEM)
+    hbm = pl.BlockSpec(memory_space=pl.ANY)
+    dma = pltpu.SemaphoreType.DMA
+    return pl.pallas_call(
+        functools.partial(kernel, cfg),
+        out_shape=jax.ShapeDtypeStruct((tok, width), BF16),
+        in_specs=[vmem] * 5 + [hbm] * 3,
+        out_specs=vmem,
+        scratch_shapes=[
+            pltpu.VMEM(w_gate.shape, BF16),
+            pltpu.VMEM(w_up.shape, BF16),
+            pltpu.VMEM(w_down.shape, BF16),
+            pltpu.VMEM((n_exp, n_ep * cap, n_ep * rows_z), BF16),
+            pltpu.VMEM((n_exp, n_ep, cap, 128), F32),
+            pltpu.VMEM((tok, n_z * rows_z), BF16),
+            pltpu.VMEM((2, tok, 128), F32),
+            pltpu.VMEM((2, 3, tok, 128), F32),
+            pltpu.VMEM((n_z, rows_z, width), BF16),
+            pltpu.VMEM((n_ep, rows_z, width), BF16),
+            pltpu.VMEM((n_exp, n_ep, cap, 2 * ff), BF16),
+            pltpu.VMEM((n_exp, 2, 2, cap, 2 * ff), BF16),
+            pltpu.VMEM((n_exp, 2, cap, 2 * ff), F32),
+            pltpu.VMEM((n_exp, 2, cap, 2 * ff), BF16),
+            pltpu.VMEM((n_exp, 2, cap, 2 * ff), BF16),
+            pltpu.VMEM((n_exp, n_ep, cap, ff), BF16),
+            pltpu.VMEM((n_z, 2, rows_z, width), F32),
+            pltpu.VMEM((n_z, rows_z, width), BF16),
+            pltpu.VMEM((n_z, rows_z, width), BF16),
+            pltpu.VMEM((n_z, rows_z, width), BF16),
+            pltpu.VMEM((n_z, rows_z, width), BF16),
+            dma((3, n_exp)),
+            dma((2, 3)),
+            dma((2, 3)),
+            dma((n_z - 1,)),
+            dma((n_z,)),
+            dma((n_ep,)),
+        ]
+        + [dma((n_exp, 2))] * 8
+        + [dma((n_z,)), dma((n_z,)), dma((n_z - 1,)), dma((n_z,))],
+        compiler_params=pltpu.CompilerParams(
+            collective_id=0, has_side_effects=True, vmem_limit_bytes=60 * 2**20
+        ),
+    )(
+        tokens,
+        in_gain.reshape(1, width),
+        out_gain.reshape(1, width),
+        routes,
+        route_weights,
+        w_gate,
+        w_up,
+        w_down,
+    )
 
 
 def run_experts(slot_rows, w_gate, w_up, w_down):
@@ -77,6 +499,9 @@
         P("ep", "tp", None),
         P("ep", None, "tp"),
     )
+    body = on_device
+    if mesh.shape["tp"] == 4 and mesh.shape["ep"] == 8:
+        body = functools.partial(fused, mesh)
     return jax.shard_map(
-        on_device, mesh=mesh, in_specs=placed, out_specs=P("ep", "tp"), check_vma=False
-    )
+        body, mesh=mesh, in_specs=placed, out_specs=P("ep", "tp"), check_vma=False
+    )

time: 186 us -> 64.1 us (0.34)
  waiting for transfers between devices: 92.3 us -> 0 us
  Pallas kernels: 0 us -> 59.2 us
  blocking collectives: 51.6 us -> 0 us
  matrix products: 15.4 us -> 0 us
  between operations: 13.5 us -> 0.01 us
  starting transfers between devices: 4.61 us -> 0 us
  other arithmetic: 3.53 us -> 0 us
    psum x1 -> x0, waiting for transfers between devices: 66.7 us -> none  [run_experts(): lax.psum(up_part, 'tp').astype(jnp.float32)]
    pallas_call x0 -> x1, Pallas kernels: none -> 59.2 us  [fused(): pl.pallas_call(functools.partial(kernel, cfg), out_shape=jax.ShapeDtypeSt...]
    all_to_all x1 -> x0, blocking collectives: 31.2 us -> none  [on_device(): lax.all_to_all(outgoing, 'ep', split_axis=0, concat_axis=0, tiled=True)]
    all_to_all x1 -> x0, waiting for transfers between devices: 25.6 us -> none  [on_device(): lax.all_to_all(answers, 'ep', split_axis=0, concat_axis=0, tiled=True)]
    psum x2 -> x0, blocking collectives: 20.3 us -> none  [the longest x1 11.4 us: on_device(): sum_squares = lax.psum(jnp.sum(values * values, axis=1), 'tp')]
    dot_general x4 -> x0, matrix products: 15.4 us -> none  [the longest x1 5.89 us: run_experts(): jnp.einsum('secf,efd->secd', active, w_down, preferred_element_type=jnp.f...]
    all_to_all x1 -> x0, starting transfers between devices: 4.61 us -> none  [on_device(): lax.all_to_all(answers, 'ep', split_axis=0, concat_axis=0, tiled=True)]
    unnamed x7 -> x3, local copies, waits for them, and re-layouts: 0.8 us -> 4.65 us
  transfers between devices with their start and end apart: 2 -> 0, of which waited for: 2 -> 0; matrix products, arithmetic and copies ran while one was open for 1% -> 0% of each run, Pallas kernels for 0% -> 0%
where the time goes in v1:
time: 64.1 us; the launch traced here: 63.8 us
  Pallas kernels  59.2 us (92%)
  local copies, waits for them, and re-layouts  4.65 us (7%)
    pallas_call x1, Pallas kernels, fused(): pl.pallas_call(functools.partial(kernel, cfg), out_shape=jax.ShapeDtypeSt...  59.2 us
    unnamed x3, local copies, waits for them, and re-layouts  4.65 us

profile of v1, /device:TPU:0, one launch (start us, length us, event | category | flops | bytes accessed | tf_op | source)
XLA Modules:
  0.0 63.8 jit_solution(495380598358486191)
XLA Ops:
  0.0 1.5 %copy.9.routes_ref = s32[512,4]{1,0:T(8,128)} copy(s32[512,4]{0,1:T(4,128)} %param.11) | data formatting | bytes 16384 | tf_op args[3]
  1.5 1.5 %copy.10.weights_ref = f32[512,4]{1,0:T(8,128)} copy(f32[512,4]{0,1:T(4,128)} %param.12) | data formatting | bytes 16384 | tf_op args[4]
  3.1 59.2 %shard_map.82 = bf16[64,1024]{1,0:T(8,128)(2,1)} custom-call(bf16[64,1024]{1,0:T(8,128)(2,1)} %tokens_ref.1, f32[1,1024]{1,0:T(1,128)} %bitcast.2, f32[1,1024]{1,0:T(1,128)} %bitcast.3, s32[512,4]{1,0:T(8,128)} %copy.9.routes_ref, f32[512,4]{1,0:T(8,128)} %copy.10.weights_ref, bf16[4,1024,1024]{2,1,0:T(8,128)(2,1)} %wg_hbm.1, bf16[4,1024,1024]{2,1,0:T(8,128)(2,1)} %wu_hbm.1, ...), custom_call_target="tpu_custom_call" | custom-call | tf_op jit(solution)/shard_map/pallas_call | solution.py:383
  62.3 1.6 %copy.12 = bf16[64,1024]{1,0:T(8,128)(2,1)} copy(bf16[64,1024]{1,0:T(8,128)(2,1)} %shard_map.82) | data formatting | bytes 262144

commit v2 on v0

--- a/solution.py
+++ b/solution.py
@@ -1,12 +1,437 @@
+import functools
+
 import jax
 import jax.numpy as jnp
 from jax import lax
+from jax.experimental import pallas as pl
+from jax.experimental.pallas import tpu as pltpu
 from jax.sharding import PartitionSpec as P
 
 D = 4096
-
+GROUP = 8
 
 EPS = 1e-06
+MESH = pl.DeviceIdType.MESH
+F32, BF16 = jnp.float32, jnp.bfloat16
+
+
+def iota(shape, dim):
+    return lax.broadcasted_iota(jnp.int32, shape, dim)
+
+
+def tdot(a, b):
+    return lax.dot_general(a, b, (((0,), (0,)), ((), ())), preferred_element_type=F32)
+
+
+def kernel(cfg, *refs):
+    n_z, tok, n_exp, cap, width, ff, top, chunks = cfg
+    it = iter(refs)
+    tokens_ref, in_gain_ref, out_gain_ref, routes_ref, weights_ref = [next(it) for _ in range(5)]
+    wg_hbm, wu_hbm, wd_hbm, out_ref, wg, wu, wd = [next(it) for _ in range(7)]
+    route_t, weight_t, pick, slot_w, own_pick = [next(it) for _ in range(5)]
+    ss_out, ss_in, send_rows, compact, x_out, x_in, r_out, r_in = [next(it) for _ in range(8)]
+    bufs = [[next(it) for _ in range(9)] for _ in chunks]
+    w_sem, ss_send, ss_recv, d_send, f_send, d_recv, f_recv = [next(it) for _ in range(7)]
+    x_send, x_recv, r_send, r_recv = [next(it) for _ in range(4)]
+    sems = [[next(it) for _ in range(8)] for _ in chunks]
+
+    rows_z = cap * GROUP // top
+    pair = 2 * tok
+    piece_cols = ff // 8
+    me = lax.axis_index("ep")
+    tp = lax.axis_index("tp")
+    z, core = me // 2, lax.rem(me, 2)
+    other = 1 - core
+    y, x = tp // 2, lax.rem(tp, 2)
+    x_tp = 2 * y + (1 - x)
+    y_tp = 2 * (1 - y) + x
+    xy_tp = 2 * (1 - y) + (1 - x)
+    partner = 2 * z + other
+    peers = (x_tp, y_tp, xy_tp)
+    chips = (z, z + 1 - 2 * lax.rem(z, 2), lax.rem(z + 2, n_z), n_z - 1 - z)
+    far_order = [d for chunk in chunks for d in chunk if d]
+
+    for j in range(n_exp):
+        pltpu.make_async_copy(wg_hbm.at[j], wg.at[j], w_sem.at[0, j]).start()
+        pltpu.make_async_copy(wu_hbm.at[j], wu.at[j], w_sem.at[1, j]).start()
+    for j in range(n_exp):
+        pltpu.make_async_copy(wd_hbm.at[j], wd.at[j], w_sem.at[2, j]).start()
+
+    def far_ep(d):
+        return 2 * chips[d] + core
+
+    barrier = pltpu.get_barrier_semaphore()
+    for peer in peers:
+        pl.semaphore_signal(barrier, inc=1, device_id={"tp": peer}, device_id_type=MESH)
+    pl.semaphore_signal(barrier, inc=1, device_id={"ep": partner}, device_id_type=MESH)
+    for d in far_order:
+        pl.semaphore_signal(barrier, inc=1, device_id={"ep": far_ep(d)}, device_id_type=MESH)
+
+    def remote(src, dst, send, recv, axis, dev):
+        return pltpu.make_async_remote_copy(
+            src_ref=src,
+            dst_ref=dst,
+            send_sem=send,
+            recv_sem=recv,
+            device_id={axis: dev},
+            device_id_type=MESH,
+        )
+
+    def square_copy(which, k):
+        return remote(
+            ss_out.at[which],
+            ss_in.at[which, k],
+            ss_send.at[which, k],
+            ss_recv.at[which, k],
+            "tp",
+            peers[k],
+        )
+
+    values = tokens_ref[...].astype(F32)
+    square = jnp.sum(values * values, axis=1, keepdims=True)
+    ss_out[0] = jnp.broadcast_to(square, (tok, 128))
+    pl.semaphore_wait(barrier, 4 + n_z - 1)
+    for k in range(3):
+        square_copy(0, k).start()
+
+    route_t[...] = routes_ref[...].T
+    weight_t[...] = weights_ref[...].T
+    lane = iota((tok, 128), 1)
+    group = route_t[pl.ds(me * tok, tok), :][:, 0:1] // GROUP
+    in_group = (lane == group).astype(F32)
+    before = (iota((tok, tok), 1) < iota((tok, tok), 0)).astype(BF16)
+    ranks = jnp.dot(before, in_group.astype(BF16), preferred_element_type=F32)
+    rank = jnp.sum(ranks * in_group, axis=1, keepdims=True).astype(jnp.int32)
+    place = jnp.where(group == chips[0], 0, -1)
+    for d in range(1, n_z):
+        place = jnp.where(group == chips[d], d, place)
+    own_lane = iota((tok, n_z * rows_z), 1)
+    own_pick[...] = (own_lane == place * rows_z + rank).astype(BF16)
+
+    def prepare(d):
+        routes = route_t[pl.ds(chips[d] * pair, pair), :]
+        weights = weight_t[pl.ds(chips[d] * pair, pair), :]
+        lane = iota((pair, 128), 1)
+        row = iota((pair, 128), 0)
+        first = me * n_exp
+        hits = jnp.where((lane == n_exp) & (routes[:, 0:1] // GROUP == z), 1.0, 0.0)
+        wt = jnp.zeros((pair, 128), F32)
+        for k in range(top):
+            match = (routes[:, k : k + 1] == first + lane) & (lane < n_exp)
+            hits = hits + jnp.where(match, 1.0, 0.0)
+            wt = wt + jnp.where(match, weights[:, k : k + 1], 0.0)
+        t_row, t_col = iota((pair, pair), 0), iota((pair, pair), 1)
+        before = ((t_col < t_row) & (t_col // tok == t_row // tok)).astype(BF16)
+        ranks = jnp.dot(before, hits.astype(BF16), preferred_element_type=F32)
+        rank = jnp.where(hits > 0.0, ranks, -1.0).astype(jnp.int32)
+        wide = iota((pair, 2 * rows_z), 1)
+        wide_core = iota((pair, 2 * rows_z), 0) // tok
+        group_rows = (
+            (rank[:, n_exp : n_exp + 1] == wide % rows_z) & (wide // rows_z == wide_core)
+        ).astype(BF16)
+        slots = n_exp * 2 * cap
+        lane = iota((pair, slots), 1)
+        row = iota((pair, slots), 0)
+        expert_rank = jnp.broadcast_to(rank[:, 0:1], (pair, slots))
+        for j in range(1, n_exp):
+            expert_rank = jnp.where(lane // (2 * cap) == j, rank[:, j : j + 1], expert_rank)
+        slot = (
+            (expert_rank == lane % cap) & ((lane // cap) % 2 == row // tok)
+        ).astype(BF16)
+        pick[d] = tdot(slot, group_rows).astype(BF16)
+        w_hi = wt.astype(BF16)
+        w_mid = (wt - w_hi.astype(F32)).astype(BF16)
+        w_lo = (wt - w_hi.astype(F32) - w_mid.astype(F32)).astype(BF16)
+        weight = tdot(slot, w_hi) + tdot(slot, w_mid) + tdot(slot, w_lo)
+        weight = jnp.where(
+            iota((slots, 128), 1) == iota((slots, 128), 0) // (2 * cap), weight, 0.0
+        )
+        weight = jnp.broadcast_to(jnp.sum(weight, axis=1, keepdims=True), (slots, 128))
+        weight = weight.reshape(n_exp, 2 * cap, 128)
+        for i, chunk in enumerate(chunks):
+            if d in chunk:
+                at = chunk.index(d) * 2 * cap
+                slot_w[i, :, at : at + 2 * cap, :] = weight
+
+    prepare(0)
+
+    for k in range(3):
+        square_copy(0, k).wait_recv()
+    square = ss_out[0] + ss_in[0, 0] + ss_in[0, 1] + ss_in[0, 2]
+    scale = lax.rsqrt(square[:, 0:1] / D + EPS)
+    normed = (values * scale * in_gain_ref[...]).astype(BF16)
+    send_rows[...] = tdot(own_pick[...], normed).astype(BF16).reshape(n_z, rows_z, width)
+
+    def dispatch(d):
+        return remote(
+            send_rows.at[d], compact.at[d, core], d_send.at[d], d_recv.at[d], "ep", far_ep(d)
+        )
+
+    def forward(d):
+        src = compact.at[d, core] if d else send_rows.at[0]
+        return remote(src, compact.at[d, core], f_send.at[d], f_recv.at[d], "ep", partner)
+
+    forward(0).start()
+    for d in far_order:
+        dispatch(d).start()
+    compact[0, core] = send_rows[0]
+
+    def side(h):
+        return (x_tp, y_tp, x, y) if h == 0 else (y_tp, x_tp, y, x)
+
+    def hop(i, stage, j, h):
+        near, next_near, a, b = side(h)
+        _, part, s1_in, _, s2_out, s2_in, act, _, _ = bufs[i]
+        send, recv = sems[i][2 * stage].at[j, h], sems[i][2 * stage + 1].at[j, h]
+        if stage == 0:
+            src, dst, to = part.at[j, pl.ds(h * 4 + 2 * (1 - a), 2)], s1_in.at[j, h], near
+        elif stage == 1:
+            src, dst, to = s2_out.at[j, h], s2_in.at[j, h], next_near
+        elif stage == 2:
+            src, to = act.at[j, h * 4 + 2 * a + b], next_near
+            dst = src
+        else:
+            src, to = act.at[j, pl.ds(h * 4 + 2 * a, 2)], near
+            dst = src
+        return remote(src, dst, send, recv, "tp", to)
+
+    def w_wait(k, j, hbm, vmem):
+        pltpu.make_async_copy(hbm.at[j], vmem.at[j], w_sem.at[k, j]).wait()
+
+    def project(i, send):
+        chunk = chunks[i]
+        xs, part = bufs[i][0], bufs[i][1]
+        for at, d in enumerate(chunk):
+            rows = compact[d].reshape(2 * rows_z, width)
+            picked = jnp.dot(pick[d], rows, preferred_element_type=F32).astype(BF16)
+            xs[:, at * 2 * cap : (at + 1) * 2 * cap, :] = picked.reshape(n_exp, 2 * cap, width)
+
+        @pl.loop(0, n_exp)
+        def _(j):
+            for k, (hbm, vmem) in enumerate(((wg_hbm, wg), (wu_hbm, wu))):
+                if i == 0:
+                    w_wait(k, j, hbm, vmem)
+                result = jnp.dot(xs[j], vmem[j], preferred_element_type=F32).astype(BF16)
+                for p in range(8):
+                    part[j, p, k] = result[:, p * piece_cols : (p + 1) * piece_cols]
+            if send:
+                for h in range(2):
+                    hop(i, 0, j, h).start()
+
+    def send_parts(i):
+        @pl.loop(0, n_exp)
+        def _(j):
+            for h in range(2):
+                hop(i, 0, j, h).start()
+
+    def add_first(i):
+        _, part, s1_in, keep, s2_out = bufs[i][:5]
+
+        @pl.loop(0, n_exp)
+        def _(j):
+            for h in range(2):
+                _, _, a, b = side(h)
+                hop(i, 0, j, h).wait_recv()
+                mine = h * 4 + 2 * a
+                s2_out[j, h] = (
+                    part[j, mine + 1 - b].astype(F32) + s1_in[j, h, 1 - b].astype(F32)
+                ).astype(BF16)
+                hop(i, 1, j, h).start()
+                keep[j, h] = part[j, mine + b].astype(F32) + s1_in[j, h, b].astype(F32)
+
+    def activate(i):
+        _, _, _, keep, _, s2_in, act = bufs[i][:7]
+        rows = act.shape[2]
+
+        @pl.loop(0, n_exp)
+        def _(j):
+            for h in range(2):
+                _, _, a, b = side(h)
+                hop(i, 1, j, h).wait_recv()
+                total = keep[j, h] + s2_in[j, h].astype(F32)
+                gate, up = total[0], total[1]
+                act[j, h * 4 + 2 * a + b] = (
+                    gate / (1.0 + jnp.exp(-gate)) * up * slot_w[i, j, 0:rows, 0:1]
+                ).astype(BF16)
+                hop(i, 2, j, h).start()
+
+    def pass_on(i):
+        @pl.loop(0, n_exp)
+        def _(j):
+            for h in range(2):
+                hop(i, 2, j, h).wait_recv()
+                hop(i, 3, j, h).start()
+
+    def swap(d):
+        return remote(x_out.at[d], x_in.at[d], x_send.at[d], x_recv.at[d], "ep", partner)
+
+    def home(d):
+        return remote(r_out.at[d], r_in.at[d], r_send.at[d], r_recv.at[d], "ep", far_ep(d))
+
+    def down(i):
+        act, res, comb = bufs[i][6:]
+
+        @pl.loop(0, n_exp)
+        def _(j):
+            if i == 0:
+                w_wait(2, j, wd_hbm, wd)
+            for h in range(2):
+                hop(i, 3, j, h).wait_recv()
+            rows = jnp.concatenate([act[j, p] for p in range(8)], axis=1)
+            res[j] = jnp.dot(rows, wd[j], preferred_element_type=F32).astype(BF16)
+
+        for at, d in enumerate(chunks[i]):
+            result = res[:, at * 2 * cap : (at + 1) * 2 * cap, :]
+            result = result.reshape(n_exp * 2 * cap, width)
+            comb[at] = tdot(pick[d], result).reshape(2, rows_z, width)
+            x_out[d] = comb[at, other].astype(BF16)
+            swap(d).start()
+
+    def send_home(i):
+        comb = bufs[i][8]
+        for at, d in enumerate(chunks[i]):
+            swap(d).wait_recv()
+            total = (comb[at, core] + x_in[d].astype(F32)).astype(BF16)
+            if d:
+                r_out[d] = total
+                home(d).start()
+            else:
+                r_in[0] = total
+
+    def received(d):
+        return remote(
+            compact.at[d, core], compact.at[d, other], f_send.at[d], f_recv.at[d], "ep", partner
+        )
+
+    received(0).wait_recv()
+    project(0, True)
+    for d in far_order:
+        prepare(d)
+    add_first(0)
+    activate(0)
+    for d in far_order:
+        dispatch(d).wait_recv()
+        forward(d).start()
+    pass_on(0)
+    for d in chunks[1]:
+        received(d).wait_recv()
+    project(1, True)
+    for d in chunks[2]:
+        received(d).wait_recv()
+    project(2, False)
+    down(0)
+    add_first(1)
+    send_home(0)
+    activate(1)
+    send_parts(2)
+    pass_on(1)
+    add_first(2)
+    activate(2)
+    down(1)
+    pass_on(2)
+    send_home(1)
+    down(2)
+    send_home(2)
+    for d in far_order:
+        home(d).wait_recv()
+
+    combined = jnp.dot(
+        own_pick[...], r_in[...].reshape(n_z * rows_z, width), preferred_element_type=F32
+    )
+    square = jnp.sum(combined * combined, axis=1, keepdims=True)
+    ss_out[1] = jnp.broadcast_to(square, (tok, 128))
+    for k in range(3):
+        square_copy(1, k).start()
+    for k in range(3):
+        square_copy(1, k).wait_recv()
+    square = ss_out[1] + ss_in[1, 0] + ss_in[1, 1] + ss_in[1, 2]
+    scale = lax.rsqrt(square[:, 0:1] / D + EPS)
+    out_ref[...] = (combined * scale * out_gain_ref[...]).astype(BF16)
+
+    for k in range(3):
+        square_copy(0, k).wait_send()
+        square_copy(1, k).wait_send()
+    for d in range(n_z):
+        forward(d).wait_send()
+        swap(d).wait_send()
+        if d:
+            dispatch(d).wait_send()
+            home(d).wait_send()
+
+    @pl.loop(0, n_exp)
+    def _(j):
+        for i in range(len(chunks)):
+            for h in range(2):
+                for stage in range(4):
+                    hop(i, stage, j, h).wait_send()
+
+
+CHUNKS = ((0,), (2, 3), (1,))
+
+
+def fused(mesh, tokens, in_gain, out_gain, routes, route_weights, w_gate, w_up, w_down):
+    tok, width = tokens.shape
+    tok_all, top = routes.shape
+    n_exp, _, ff = w_gate.shape
+    n_ep = mesh.shape["ep"]
+    n_z = n_ep // 2
+    cap = max(2, 2 * tok * top // (n_exp * n_ep))
+    rows_z = cap * GROUP // top
+    cfg = (n_z, tok, n_exp, cap, width, ff, top, CHUNKS)
+    vmem = pl.BlockSpec(memory_space=pltpu.VMEM)
+    hbm = pl.BlockSpec(memory_space=pl.ANY)
+    dma = pltpu.SemaphoreType.DMA
+    longest = max(len(chunk) for chunk in CHUNKS)
+    scratch = [
+        pltpu.VMEM(w_gate.shape, BF16),
+        pltpu.VMEM(w_up.shape, BF16),
+        pltpu.VMEM(w_down.shape, BF16),
+        pltpu.VMEM((tok_all, top), jnp.int32),
+        pltpu.VMEM((tok_all, top), F32),
+        pltpu.VMEM((n_z, n_exp * 2 * cap, 2 * rows_z), BF16),
+        pltpu.VMEM((len(CHUNKS), n_exp, longest * 2 * cap, 128), F32),
+        pltpu.VMEM((tok, n_z * rows_z), BF16),
+        pltpu.VMEM((2, tok, 128), F32),
+        pltpu.VMEM((2, 3, tok, 128), F32),
+        pltpu.VMEM((n_z, rows_z, width), BF16),
+        pltpu.VMEM((n_z, 2, rows_z, width), BF16),
+    ] + [pltpu.VMEM((n_z, rows_z, width), BF16)] * 4
+    for chunk in CHUNKS:
+        rows = len(chunk) * 2 * cap
+        cols = ff // 8
+        scratch += [
+            pltpu.VMEM((n_exp, rows, width), BF16),
+            pltpu.VMEM((n_exp, 8, 2, rows, cols), BF16),
+            pltpu.VMEM((n_exp, 2, 2, 2, rows, cols), BF16),
+            pltpu.VMEM((n_exp, 2, 2, rows, cols), F32),
+            pltpu.VMEM((n_exp, 2, 2, rows, cols), BF16),
+            pltpu.VMEM((n_exp, 2, 2, rows, cols), BF16),
+            pltpu.VMEM((n_exp, 8, rows, cols), BF16),
+            pltpu.VMEM((n_exp, rows, width), BF16),
+            pltpu.VMEM((len(chunk), 2, rows_z, width), F32),
+        ]
+    scratch += [dma((3, n_exp)), dma((2, 3)), dma((2, 3))]
+    scratch += [dma((n_z,))] * 8
+    scratch += [dma((n_exp, 2))] * (8 * len(CHUNKS))
+    return pl.pallas_call(
+        functools.partial(kernel, cfg),
+        out_shape=jax.ShapeDtypeStruct((tok, width), BF16),
+        in_specs=[vmem] * 5 + [hbm] * 3,
+        out_specs=vmem,
+        scratch_shapes=scratch,
+        compiler_params=pltpu.CompilerParams(
+            collective_id=0, has_side_effects=True, vmem_limit_bytes=60 * 2**20
+        ),
+    )(
+        tokens,
+        in_gain.reshape(1, width),
+        out_gain.reshape(1, width),
+        routes.T,
+        route_weights.T,
+        w_gate,
+        w_up,
+        w_down,
+    )
 
 
 def run_experts(slot_rows, w_gate, w_up, w_down):
@@ -77,6 +502,9 @@
         P("ep", "tp", None),
         P("ep", None, "tp"),
     )
+    body = on_device
+    if mesh.shape["tp"] == 4 and mesh.shape["ep"] == 8:
+        body = functools.partial(fused, mesh)
     return jax.shard_map(
-        on_device, mesh=mesh, in_specs=placed, out_specs=P("ep", "tp"), check_vma=False
-    )
+        body, mesh=mesh, in_specs=placed, out_specs=P("ep", "tp"), check_vma=False
+    )

time: 186 us -> 66.1 us (0.36)
  waiting for transfers between devices: 92.3 us -> 0 us
  Pallas kernels: 0 us -> 64.4 us
  blocking collectives: 51.6 us -> 0 us
  matrix products: 15.4 us -> 0 us
  between operations: 13.5 us -> 0.01 us
  starting transfers between devices: 4.61 us -> 0 us
  other arithmetic: 3.53 us -> 0 us
  local copies, waits for them, and re-layouts: 5.01 us -> 1.57 us
    psum x1 -> x0, waiting for transfers between devices: 66.7 us -> none  [run_experts(): lax.psum(up_part, 'tp').astype(jnp.float32)]
    pallas_call x0 -> x1, Pallas kernels: none -> 64.4 us  [fused(): pl.pallas_call(functools.partial(kernel, cfg), out_shape=jax.ShapeDtypeSt...]
    all_to_all x1 -> x0, blocking collectives: 31.2 us -> none  [on_device(): lax.all_to_all(outgoing, 'ep', split_axis=0, concat_axis=0, tiled=True)]
    all_to_all x1 -> x0, waiting for transfers between devices: 25.6 us -> none  [on_device(): lax.all_to_all(answers, 'ep', split_axis=0, concat_axis=0, tiled=True)]
    psum x2 -> x0, blocking collectives: 20.3 us -> none  [the longest x1 11.4 us: on_device(): sum_squares = lax.psum(jnp.sum(values * values, axis=1), 'tp')]
    dot_general x4 -> x0, matrix products: 15.4 us -> none  [the longest x1 5.89 us: run_experts(): jnp.einsum('secf,efd->secd', active, w_down, preferred_element_type=jnp.f...]
    all_to_all x1 -> x0, starting transfers between devices: 4.61 us -> none  [on_device(): lax.all_to_all(answers, 'ep', split_axis=0, concat_axis=0, tiled=True)]
    reduce_sum x4 -> x0, other arithmetic: 1.96 us -> none  [the longest x1 1.03 us: on_device(): sum_squares = lax.psum(jnp.sum(values * values, axis=1), 'tp')]
  transfers between devices with their start and end apart: 2 -> 0, of which waited for: 2 -> 0; matrix products, arithmetic and copies ran while one was open for 1% -> 0% of each run, Pallas kernels for 0% -> 0%
where the time goes in v2:
time: 66.1 us; the launch traced here: 65.9 us
  Pallas kernels  64.4 us (97%)
  local copies, waits for them, and re-layouts  1.57 us (2%)
    pallas_call x1, Pallas kernels, fused(): pl.pallas_call(functools.partial(kernel, cfg), out_shape=jax.ShapeDtypeSt...  64.4 us
    unnamed x1, local copies, waits for them, and re-layouts  1.57 us

profile of v2, /device:TPU:0, one launch (start us, length us, event | category | flops | bytes accessed | tf_op | source)
XLA Modules:
  0.0 65.9 jit_solution(14147150838697025035)
XLA Ops:
  0.0 64.4 %shard_map.82 = bf16[64,1024]{1,0:T(8,128)(2,1)} custom-call(bf16[64,1024]{1,0:T(8,128)(2,1)} %refs_0_.1, f32[1,1024]{1,0:T(1,128)} %bitcast.6, f32[1,1024]{1,0:T(1,128)} %bitcast.7, s32[4,512]{1,0:T(4,128)} %bitcast.4, f32[4,512]{1,0:T(4,128)} %bitcast.5, bf16[4,1024,1024]{2,1,0:T(8,128)(2,1)} %refs_5_.1, bf16[4,1024,1024]{2,1,0:T(8,128)(2,1)} %refs_6_.1, ...), custom_call_target="tpu_custom_call" | custom-call | tf_op jit(solution)/shard_map/pallas_call | solution.py:416
  64.4 1.6 %copy.10 = bf16[64,1024]{1,0:T(8,128)(2,1)} copy(bf16[64,1024]{1,0:T(8,128)(2,1)} %shard_map.82) | data formatting | bytes 262144

commit v3 on v2

--- a/solution.py
+++ b/solution.py
@@ -49,7 +49,7 @@
     partner = 2 * z + other
     peers = (x_tp, y_tp, xy_tp)
     chips = (z, z + 1 - 2 * lax.rem(z, 2), lax.rem(z + 2, n_z), n_z - 1 - z)
-    far_order = [d for chunk in chunks for d in chunk if d]
+    far_order = range(1, n_z)
 
     for j in range(n_exp):
         pltpu.make_async_copy(wg_hbm.at[j], wg.at[j], w_sem.at[0, j]).start()
@@ -198,7 +198,7 @@
     def w_wait(k, j, hbm, vmem):
         pltpu.make_async_copy(hbm.at[j], vmem.at[j], w_sem.at[k, j]).wait()
 
-    def project(i, send):
+    def project(i):
         chunk = chunks[i]
         xs, part = bufs[i][0], bufs[i][1]
         for at, d in enumerate(chunk):
@@ -214,13 +214,6 @@
                 result = jnp.dot(xs[j], vmem[j], preferred_element_type=F32).astype(BF16)
                 for p in range(8):
                     part[j, p, k] = result[:, p * piece_cols : (p + 1) * piece_cols]
-            if send:
-                for h in range(2):
-                    hop(i, 0, j, h).start()
-
-    def send_parts(i):
-        @pl.loop(0, n_exp)
-        def _(j):
             for h in range(2):
                 hop(i, 0, j, h).start()
 
@@ -303,35 +296,41 @@
             compact.at[d, core], compact.at[d, other], f_send.at[d], f_recv.at[d], "ep", partner
         )
 
-    received(0).wait_recv()
-    project(0, True)
-    for d in far_order:
-        prepare(d)
-    add_first(0)
-    activate(0)
-    for d in far_order:
+    def relay(d):
         dispatch(d).wait_recv()
         forward(d).start()
-    pass_on(0)
-    for d in chunks[1]:
+
+    own, far, near = range(3)
+    received(0).wait_recv()
+    project(own)
+    for d in chunks[near]:
+        prepare(d)
+        relay(d)
+    add_first(own)
+    for d in chunks[near]:
         received(d).wait_recv()
-    project(1, True)
-    for d in chunks[2]:
+    project(near)
+    for d in chunks[far]:
+        prepare(d)
+    activate(own)
+    for d in chunks[far]:
+        relay(d)
+    for d in chunks[far]:
         received(d).wait_recv()
-    project(2, False)
-    down(0)
-    add_first(1)
-    send_home(0)
-    activate(1)
-    send_parts(2)
-    pass_on(1)
-    add_first(2)
-    activate(2)
-    down(1)
-    pass_on(2)
-    send_home(1)
-    down(2)
-    send_home(2)
+    project(far)
+    pass_on(own)
+    add_first(near)
+    add_first(far)
+    activate(near)
+    down(own)
+    activate(far)
+    pass_on(far)
+    send_home(own)
+    pass_on(near)
+    down(far)
+    send_home(far)
+    down(near)
+    send_home(near)
     for d in far_order:
         home(d).wait_recv()
 

time: 66.1 us -> 64.4 us (0.974)
  Pallas kernels: 64.4 us -> 62.7 us
    pallas_call x1, Pallas kernels: 64.4 us -> 62.7 us  [fused(): pl.pallas_call(functools.partial(kernel, cfg), out_shape=jax.ShapeDtypeSt...]
where the time goes in v3:
time: 64.4 us; the launch traced here: 64.3 us
  Pallas kernels  62.7 us (97%)
  local copies, waits for them, and re-layouts  1.57 us (2%)
    pallas_call x1, Pallas kernels, fused(): pl.pallas_call(functools.partial(kernel, cfg), out_shape=jax.ShapeDtypeSt...  62.7 us
    unnamed x1, local copies, waits for them, and re-layouts  1.57 us

profile of v3, /device:TPU:0, one launch (start us, length us, event | category | flops | bytes accessed | tf_op | source)
XLA Modules:
  0.0 64.3 jit_solution(11347202359792897603)
XLA Ops:
  0.0 62.7 %shard_map.82 = bf16[64,1024]{1,0:T(8,128)(2,1)} custom-call(bf16[64,1024]{1,0:T(8,128)(2,1)} %refs_0_.1, f32[1,1024]{1,0:T(1,128)} %bitcast.6, f32[1,1024]{1,0:T(1,128)} %bitcast.7, s32[4,512]{1,0:T(4,128)} %bitcast.4, f32[4,512]{1,0:T(4,128)} %bitcast.5, bf16[4,1024,1024]{2,1,0:T(8,128)(2,1)} %refs_5_.1, bf16[4,1024,1024]{2,1,0:T(8,128)(2,1)} %refs_6_.1, ...), custom_call_target="tpu_custom_call" | custom-call | tf_op jit(solution)/shard_map/pallas_call | solution.py:415
  62.7 1.6 %copy.10 = bf16[64,1024]{1,0:T(8,128)(2,1)} copy(bf16[64,1024]{1,0:T(8,128)(2,1)} %shard_map.82) | data formatting | bytes 262144
